TPU v7x, 256 devices: a whole 4x4x8 slice. The times are simulated.
256 devices in a mesh: sp: 64 (over z, x, core), tp: 4 (over y).
Axes of the slice: x: 4, y: 4, z: 8, core: 2. Of those that a mesh axis runs over, the one named last changes fastest.
Arguments:
- residual: bfloat16 [16384, 2048], P('sp', 'tp'), may hold values from -8 to 8
- query_latent: bfloat16 [16384, 512], P('sp'), may hold values from -6 to 6
- shared_latent: bfloat16 [16384, 256], P('sp'), may hold values from -6 to 6
- rotary_key: bfloat16 [16384, 32], P('sp'), may hold values from -300 to 300
- query_gain: float32 [512], replicated, may hold values from 0.1 to 1.9
- latent_gain: float32 [256], replicated, may hold values from 0.1 to 1.9
- query_narrow: bfloat16 [512, 384], P(None, 'tp'), may hold values from -0.5 to 0.5
- key_narrow: bfloat16 [256, 256], P(None, 'tp'), may hold values from -0.375 to 0.375
- value_narrow: bfloat16 [256, 256], P(None, 'tp'), may hold values from -0.375 to 0.375
- query_wide: bfloat16 [512, 640], P(None, 'tp'), may hold values from -0.5 to 0.5
- key_wide: bfloat16 [256, 512], P(None, 'tp'), may hold values from -0.375 to 0.375
- value_wide: bfloat16 [256, 512], P(None, 'tp'), may hold values from -0.375 to 0.375
- output_narrow: bfloat16 [256, 2048], P('tp'), may hold values from -1.75 to 1.75
- output_wide: bfloat16 [512, 2048], P('tp'), may hold values from -1.75 to 1.75
- first_gain: float32 [2048], P('tp'), may hold values from 0.1 to 1.9
- first_bias: float32 [2048], P('tp'), may hold values from -1.5 to 1.5
- gate_weight: bfloat16 [2048, 5632], P('sp', 'tp'), may hold values from -0.125 to 0.125
- up_weight: bfloat16 [2048, 5632], P('sp', 'tp'), may hold values from -0.125 to 0.125
- down_weight: bfloat16 [5632, 2048], P('tp', 'sp'), may hold values from -0.078125 to 0.078125
- second_gain: float32 [2048], P('tp'), may hold values from 0.1 to 1.9
- second_bias: float32 [2048], P('tp'), may hold values from -1.5 to 1.5
Outputs:
- layer_out: bfloat16 [16384, 2048], P('sp', 'tp')
All inputs are finite; a program needn't handle non-finite values.
Results may differ from a plain program's by a relative error of at most 0.017.
The roundings to bfloat16 on the way count: a program that leaves them out, or rounds other values in their place, can miss the bound.
Values may be sent and summed in bfloat16 or wider, within the bound.
A program may use at most 192 MiB of HBM per device.

v0:
```python
import jax
import jax.numpy as jnp
from jax import lax
from jax.sharding import PartitionSpec as P

ROPE = 32
NOPE_A = 64
V_A = 64
NOPE_B = 128
V_B = 128
GRID_W = 64
EPS_ROOT = 1e-06
EPS_LAYER = 1e-05
THETA = 10000.0
DEEP_ALPHA = 2.0**0.25


def in_one_piece(arrays, axis, dim, along):
    ends, at = ([], 0)
    for a in arrays[:-1]:
        at += a.shape[along]
        ends.append(at)
    both = jnp.concatenate(arrays, axis=along)
    return tuple(jnp.split(lax.all_gather(both, axis, axis=dim, tiled=True), ends, axis=along))


def split_up(x, dim, size):
    before, after = (x.shape[:dim], x.shape[dim + 1 :])
    return jnp.moveaxis(x.reshape(*before, size, -1, *after), dim, 0)


def sum_at_owner(x, axis, dim):
    size = lax.axis_size(axis)
    pieces = lax.all_to_all(split_up(x, dim, size), axis, 0, 0, tiled=True)
    return jnp.sum(pieces.astype(jnp.float32), axis=0)


def sent_to_all(x, axis):
    copies = jnp.broadcast_to(x, (lax.axis_size(axis), *x.shape))
    return lax.all_to_all(copies, axis, split_axis=0, concat_axis=0, tiled=True)


def of_everyone(x, axis):
    return sent_to_all(x, axis).sum(axis=0)


def in_one(arrays, axis):
    ends = [0]
    for a in arrays:
        ends.append(ends[-1] + a.size)
    so_far = of_everyone(jnp.concatenate([a.ravel() for a in arrays]), axis)
    return tuple((so_far[b:e].reshape(a.shape) for a, b, e in zip(arrays, ends, ends[1:])))


def in_order(pieces, dim):
    shape = list(pieces.shape[1:])
    shape[dim] *= pieces.shape[0]
    return jnp.moveaxis(pieces, 0, dim).reshape(shape)


def collect(x, axis, dim):
    return in_order(sent_to_all(x, axis), dim)


def rotate(half_part, angle):
    lower, upper = jnp.split(half_part, 2, axis=-1)
    cosine = jnp.cos(angle)
    sine = jnp.sin(angle)
    return jnp.concatenate([lower * cosine - upper * sine, upper * cosine + lower * sine], axis=-1)


def turn_axial(values_in, positions):
    quarter = values_in.shape[-1] // 4
    freqs = THETA ** (-(2.0 * jnp.arange(quarter, dtype=jnp.float32)) / (2 * quarter))
    row_angle = (positions // GRID_W).astype(jnp.float32)[:, None, None] * freqs
    col_angle = (positions % GRID_W).astype(jnp.float32)[:, None, None] * freqs
    first_half, second_half = jnp.split(values_in, 2, axis=-1)
    return jnp.concatenate([rotate(first_half, row_angle), rotate(second_half, col_angle)], axis=-1)


def root_scale(latent, gain):
    floated = latent.astype(jnp.float32)
    return (
        floated * lax.rsqrt(jnp.mean(floated * floated, axis=-1, keepdims=True) + EPS_ROOT) * gain
    )


def make_query(normed, weight, plain_dim, positions):
    product = jnp.dot(normed, weight, preferred_element_type=jnp.float32)
    head_count = weight.shape[1] // (plain_dim + ROPE)
    product = product.reshape(product.shape[0], head_count, plain_dim + ROPE)
    turned = turn_axial(product[:, :, plain_dim:], positions)
    return jnp.concatenate([product[:, :, :plain_dim], turned], axis=-1).astype(jnp.bfloat16)


def fresh_state(row_count, head_count, value_dim):
    largest = jnp.full((head_count, row_count), -jnp.inf, jnp.float32)
    totals = jnp.zeros((head_count, row_count), jnp.float32)
    weighted = jnp.zeros((row_count, head_count, value_dim), jnp.float32)
    return (largest, totals, weighted)


def update(state_now, queries, key_rows, value_rows, rotary_rows, plain_dim):
    largest, totals, weighted = state_now
    score_scale = queries.shape[2] ** (-0.5)
    scores = jnp.einsum(
        "qhd,khd->hqk", queries[:, :, :plain_dim], key_rows, preferred_element_type=jnp.float32
    )
    scores = scores + jnp.einsum(
        "qhd,kd->hqk", queries[:, :, plain_dim:], rotary_rows, preferred_element_type=jnp.float32
    )
    scores = scores * score_scale
    new_largest = jnp.max(scores, axis=-1)
    factor = jnp.exp(largest - new_largest)
    raised = jnp.exp(scores - new_largest[:, :, None])
    totals = totals * factor + jnp.sum(raised, axis=-1)
    added = jnp.einsum(
        "hqk,khd->qhd", raised.astype(jnp.bfloat16), value_rows, preferred_element_type=jnp.float32
    )
    weighted = weighted * factor.T[:, :, None] + added
    return (new_largest, totals, weighted)


def finish(state_now):
    largest, totals, weighted = state_now
    output = (weighted / totals.T[:, :, None]).astype(jnp.bfloat16)
    return output.reshape(output.shape[0], output.shape[1] * output.shape[2])


def finish_norm(summed, sums, squares, gain, bias, width_total):
    center = sums / width_total
    spread = squares / width_total - center * center
    normed = (summed - center[:, None]) * lax.rsqrt(spread + EPS_LAYER)[:, None]
    return (normed * gain + bias).astype(jnp.bfloat16)


def body(
    residual,
    query_latent,
    shared_latent,
    rotary_key,
    query_gain,
    latent_gain,
    query_narrow,
    key_narrow,
    value_narrow,
    query_wide,
    key_wide,
    value_wide,
    output_narrow,
    output_wide,
    first_gain,
    first_bias,
    gate_weight,
    up_weight,
    down_weight,
    second_gain,
    second_bias,
):
    row_count = residual.shape[0]
    offset = lax.axis_index("sp") * row_count
    positions = offset + jnp.arange(row_count, dtype=jnp.int32)
    query_normed = root_scale(query_latent, query_gain).astype(jnp.bfloat16)
    narrow_queries = make_query(query_normed, query_narrow, NOPE_A, positions)
    wide_queries = make_query(query_normed, query_wide, NOPE_B, positions)
    narrow_heads = narrow_queries.shape[1]
    wide_heads = wide_queries.shape[1]
    start_state = (
        fresh_state(row_count, narrow_heads, V_A),
        fresh_state(row_count, wide_heads, V_B),
    )
    shard_rows = in_one_piece((shared_latent, rotary_key), "sp", 0, 1)
    latent_rows = shard_rows[0]
    normed = root_scale(latent_rows, latent_gain).astype(jnp.bfloat16)
    count = latent_rows.shape[0]
    narrow_keys = jnp.dot(normed, key_narrow, preferred_element_type=jnp.float32).astype(
        jnp.bfloat16
    )
    narrow_vals = jnp.dot(normed, value_narrow, preferred_element_type=jnp.float32).astype(
        jnp.bfloat16
    )
    wide_keys = jnp.dot(normed, key_wide, preferred_element_type=jnp.float32).astype(jnp.bfloat16)
    wide_vals = jnp.dot(normed, value_wide, preferred_element_type=jnp.float32).astype(jnp.bfloat16)
    key_positions = jnp.arange(count, dtype=jnp.int32)
    rotated = turn_axial(shard_rows[1].astype(jnp.float32)[:, None, :], key_positions)[
        :, 0, :
    ].astype(jnp.bfloat16)
    count = rotated.shape[0]
    narrow_state = update(
        start_state[0],
        narrow_queries,
        narrow_keys.reshape(count, narrow_heads, NOPE_A),
        narrow_vals.reshape(count, narrow_heads, V_A),
        rotated,
        NOPE_A,
    )
    wide_state = update(
        start_state[1],
        wide_queries,
        wide_keys.reshape(count, wide_heads, NOPE_B),
        wide_vals.reshape(count, wide_heads, V_B),
        rotated,
        NOPE_B,
    )
    narrow_out = finish(narrow_state)
    wide_out = finish(wide_state)
    terms = jnp.dot(narrow_out, output_narrow, preferred_element_type=jnp.float32)
    terms = terms + jnp.dot(wide_out, output_wide, preferred_element_type=jnp.float32)
    mixed = sum_at_owner(terms.astype(jnp.bfloat16), "tp", 1)
    width_total = mixed.shape[1] * lax.axis_size("tp")
    summed = DEEP_ALPHA * residual.astype(jnp.float32) + mixed
    sums, squares = in_one((jnp.sum(summed, axis=1), jnp.sum(summed * summed, axis=1)), "tp")
    normed_first = finish_norm(summed, sums, squares, first_gain, first_bias, width_total)
    full_rows = collect(normed_first, "tp", 1)
    shard_rows = in_one_piece((gate_weight, up_weight), "sp", 0, 1)
    gate_part = jnp.dot(full_rows, shard_rows[0], preferred_element_type=jnp.float32)
    lifted_part = jnp.dot(full_rows, shard_rows[1], preferred_element_type=jnp.float32)
    hidden = (jax.nn.silu(gate_part) * lifted_part).astype(jnp.bfloat16)
    feed_terms = jnp.dot(
        hidden,
        lax.all_gather(down_weight, "sp", axis=1, tiled=True),
        preferred_element_type=jnp.float32,
    )
    feed = sum_at_owner(feed_terms.astype(jnp.bfloat16), "tp", 1)
    summed_two = DEEP_ALPHA * normed_first.astype(jnp.float32) + feed
    sums_two, squares_two = in_one(
        (jnp.sum(summed_two, axis=1), jnp.sum(summed_two * summed_two, axis=1)), "tp"
    )
    return finish_norm(summed_two, sums_two, squares_two, second_gain, second_bias, width_total)


def solution(mesh):
    return jax.shard_map(
        body,
        mesh=mesh,
        in_specs=(
            P("sp", "tp"),
            P("sp", None),
            P("sp", None),
            P("sp", None),
            P(),
            P(),
            P(None, "tp"),
            P(None, "tp"),
            P(None, "tp"),
            P(None, "tp"),
            P(None, "tp"),
            P(None, "tp"),
            P("tp", None),
            P("tp", None),
            P("tp"),
            P("tp"),
            P("sp", "tp"),
            P("sp", "tp"),
            P("tp", "sp"),
            P("tp"),
            P("tp"),
        ),
        out_specs=P("sp", "tp"),
        check_vma=False,
    )
```

profile of v0, /device:TPU:8, one launch (start us, length us, event | category | flops | bytes accessed | tf_op | source)
XLA Modules:
  0.0 313.4 jit_solution(8049191181758371652)
XLA Ops:
  6.5 1.1 copy.41
  7.6 1.4 pad_maximum_fusion.4
  9.1 1.6 pad_maximum_fusion.1
  10.8 0.7 all-gather.8.cloned.1.call-update
  11.5 1.1 fusion.72
  12.6 1.3 convolution_bitcast_fusion.4
  13.9 1.3 convolution_bitcast_fusion.5
  15.4 84.6 %all-gather.4.cloned.1.call-done = bf16[16384,288]{0,1:T(8,128)(2,1)} async-done(((bf16[256,288]{0,1:T(8,128)(2,1)}), bf16[16384,288]{0,1:T(8,128)(2,1)}) %all-gather.4.cloned.1.call-update) | async-done | bytes 9437200 | tf_op jit(solution)/shard_map/all_gather | solution.py:24
  99.9 5.1 %fusion.4 = f32[16384]{0:T(1024)S(1)} fusion(bf16[16384,288]{0,1:T(8,128)(2,1)} %all-gather.4.cloned.1.call-done), kind=kLoop, calls=%fused_computation.14 | loop fusion | flops 12566528 | bytes 8454144 | tf_op jit(solution)/shard_map/reduce_sum | solution.py:84
  105.1 1.4 fusion.62
  106.5 4.4 %fusion.84 = (bf16[16384,8]{0,1:T(8,128)(2,1)S(1)}, bf16[16384,8]{0,1:T(8,128)(2,1)S(1)}, bf16[16384,8]{0,1:T(8,128)(2,1)S(1)}, bf16[16384,8]{0,1:T(8,128)(2,1)S(1)}) fusion(f32[16384,1,32]{0,2,1:T(8,128)S(1)} %fusion.62, f32[8]{0:T(128)S(1)} %multiply_power_fusion, f32[16384]{0:T(1024)S(1)} %get-tuple-element.43, f32[16384]{0:T(1024)S(1)} %get-tuple-element.44), kind=kLoop, calls=%fused_computation.90 | loop fusion | flops 2359296 | bytes 3276832 | tf_op jit(solution)/shard_map/concatenate | solution.py:78
  110.9 8.1 %convolution_bitcast_fusion.2 = f32[1,256,16384]{2,1,0:T(8,128)} fusion(bf16[16384,8]{0,1:T(8,128)(2,1)S(1)} %get-tuple-element.13, bf16[16384,8]{0,1:T(8,128)(2,1)S(1)} %get-tuple-element.14, bf16[16384,8]{0,1:T(8,128)(2,1)S(1)} %get-tuple-element.10, bf16[16384,8]{0,1:T(8,128)(2,1)S(1)} %get-tuple-element.9, bf16[256,1,8]{0,2,1:T(8,128)(2,1)S(1)} %get-tuple-element.25, ...), kind=kOutput, calls=%fused_computation.2 | convolution fusion | flops 272695296 | bytes 17842176 | tf_op jit(solution)/shard_map/qhd,kd->hqk/dot_general | solution.py:109
  119.0 14.3 %fusion.167 = (f32[256]{0:T(256)S(1)}, f32[1,256,16384]{2,1,0:T(8,128)}) fusion(f32[1,256,16384]{2,1,0:T(8,128)} %convolution_bitcast_fusion.2, bf16[256,64]{0,1:T(8,128)(2,1)S(1)} %copy-done.4, f32[256]{0:T(256)S(1)} %copy-done.5, f32[16384]{0:T(1024)S(1)} %add_rsqrt_fusion, bf16[16384,288]{0,1:T(8,128)(2,1)} %all-gather.4.cloned.1.call-done, ...), kind=kOutput, calls=%fused_computation.191 | convolution fusion | flops 1104150272 | bytes 42076160 | tf_op jit(solution)/shard_map/qhd,khd->hqk/dot_general | solution.py:106
  133.3 8.1 %convolution_bitcast_fusion = f32[1,256,16384]{2,1,0:T(8,128)} fusion(bf16[16384,8]{0,1:T(8,128)(2,1)S(1)} %get-tuple-element.13, bf16[16384,8]{0,1:T(8,128)(2,1)S(1)} %get-tuple-element.14, bf16[16384,8]{0,1:T(8,128)(2,1)S(1)} %get-tuple-element.10, bf16[16384,8]{0,1:T(8,128)(2,1)S(1)} %get-tuple-element.9, bf16[256,1,8]{0,2,1:T(8,128)(2,1)S(1)} %get-tuple-element.28, ...), kind=kOutput, calls=%fused_computation | convolution fusion | flops 272695296 | bytes 17842176 | tf_op jit(solution)/shard_map/qhd,kd->hqk/dot_general | solution.py:109
  141.4 8.2 %fusion.7 = f32[256]{0:T(256)S(1)} fusion(f32[1,256,16384]{2,1,0:T(8,128)} %get-tuple-element.42, f32[256]{0:T(256)S(1)} %get-tuple-element.41), kind=kLoop, calls=%fused_computation.19 | loop fusion | flops 8388352 | bytes 16779264 | tf_op jit(solution)/shard_map/reduce_sum | solution.py:116
  149.6 15.2 %fusion.164 = (f32[256]{0:T(256)S(1)}, f32[1,256,16384]{2,1,0:T(8,128)}) fusion(f32[1,256,16384]{2,1,0:T(8,128)} %convolution_bitcast_fusion, bf16[256,128]{1,0:T(8,128)(2,1)S(1)} %copy-done.3, f32[256]{0:T(256)S(1)} %copy-done.5, f32[16384]{0:T(1024)S(1)} %add_rsqrt_fusion, bf16[16384,288]{0,1:T(8,128)(2,1)} %all-gather.4.cloned.1.call-done, ...), kind=kOutput, calls=%fused_computation.190 | convolution fusion | flops 2178940672 | bytes 42141696 | tf_op jit(solution)/shard_map/qhd,khd->hqk/dot_general | solution.py:106
  164.8 8.5 %fusion.9 = f32[256]{0:T(256)S(1)} fusion(f32[1,256,16384]{2,1,0:T(8,128)} %get-tuple-element.40, f32[256]{0:T(256)S(1)} %get-tuple-element.39), kind=kLoop, calls=%fused_computation.21 | loop fusion | flops 8388352 | bytes 16779264 | tf_op jit(solution)/shard_map/reduce_sum | solution.py:116
  173.4 12.0 %fusion.44 = bf16[256,128]{0,1:T(8,128)(2,1)S(1)} fusion(f32[1,256,16384]{2,1,0:T(8,128)} %get-tuple-element.40, f32[256]{0:T(256)S(1)} %get-tuple-element.39, bf16[256,128]{1,0:T(8,128)(2,1)S(1)} %copy-done.10, f32[256]{0:T(256)S(1)} %get-tuple-element.38, f32[256]{0:T(256)S(1)} %get-tuple-element.37, f32[256]{0:T(256)S(1)} %copy-done.5, ...), kind=kOutput, calls=%fused_computation.46 | convolution fusion | flops 2174844928 | bytes 25366528 | tf_op jit(solution)/shard_map/hqk,khd->qhd/dot_general | solution.py:117
  185.4 0.5 fusion.170
  185.8 11.3 %fusion.59 = bf16[256,64]{0,1:T(8,128)(2,1)S(1)} fusion(f32[1,256,16384]{2,1,0:T(8,128)} %get-tuple-element.42, f32[256]{0:T(256)S(1)} %get-tuple-element.41, bf16[256,64]{0,1:T(8,128)(2,1)S(1)} %copy-done.11, f32[256]{0:T(256)S(1)} %get-tuple-element.36, f32[256]{0:T(256)S(1)} %get-tuple-element.35, f32[256]{0:T(256)S(1)} %copy-done.5, ...), kind=kOutput, calls=%fused_computation.51 | convolution fusion | flops 1100005376 | bytes 25300992 | tf_op jit(solution)/shard_map/hqk,khd->qhd/dot_general | solution.py:117
  197.2 0.5 fusion.26
  197.7 18.6 %all_to_all.27 = bf16[4,256,512]{2,1,0:T(8,128)(2,1)S(1)} all-to-all(bf16[4,256,512]{2,1,0:T(8,128)(2,1)S(1)} %bitcast.138), channel_id=1, replica_groups=mesh['sp'=64,'tp'=4] {'tp'}, dimensions={0} | all-to-all | bytes 2097152 | tf_op jit(solution)/shard_map/all_to_all | solution.py:34
  216.5 0.2 fusion.87
  216.8 7.7 %all_to_all.28 = f32[4,1,512]{2,1,0:T(1,128)S(1)} all-to-all(f32[4,1,512]{2,1,0:T(1,128)S(1)} %broadcast_in_dim.16), channel_id=1, replica_groups=mesh['sp'=64,'tp'=4] {'tp'}, dimensions={0} | all-to-all | bytes 16384 | tf_op jit(solution)/shard_map/all_to_all | solution.py:40
  224.9 15.6 %all_to_all.29 = bf16[4,256,512]{1,2,0:T(8,128)(2,1)S(1)} all-to-all(bf16[4,256,512]{1,2,0:T(8,128)(2,1)S(1)} %broadcast_in_dim.17), channel_id=1, replica_groups=mesh['sp'=64,'tp'=4] {'tp'}, dimensions={0} | all-to-all | bytes 2097152 | tf_op jit(solution)/shard_map/all_to_all | solution.py:40
  240.5 5.6 %fusion.21 = f32[256,1408]{1,0:T(8,128)} fusion(bf16[256,2048]{0,1:T(8,128)(2,1)S(1)} %bitcast.140, bf16[2048,2816]{1,0:T(8,128)(2,1)} %all-gather.6.cloned.1.call-done), kind=kOutput, calls=%fused_computation.31 | convolution fusion | flops 1476395008 | bytes 8257536 | tf_op jit(solution)/shard_map/dot_general | solution.py:216
  246.1 24.8 %all-gather.8.cloned.1.call-done = bf16[1408,2048]{0,1:T(8,128)(2,1)} async-done(((bf16[1408,32]{0,1:T(8,128)(2,1)}), bf16[1408,2048]{0,1:T(8,128)(2,1)}) %all-gather.8.cloned.1.call-update) | async-done | bytes 5767184 | tf_op jit(solution)/shard_map/all_gather | solution.py:221
  270.9 8.3 %convolution_convert_fusion.4 = bf16[256,2048]{1,0:T(8,128)(2,1)S(1)} fusion(bf16[1408,2048]{0,1:T(8,128)(2,1)} %all-gather.8.cloned.1.call-done, bf16[256,2048]{0,1:T(8,128)(2,1)S(1)} %bitcast.141, bf16[2048,2816]{1,0:T(8,128)(2,1)} %all-gather.6.cloned.1.call-done, f32[256,1408]{1,0:T(8,128)} %fusion.21), kind=kOutput, calls=%fused_computation.37 | convolution fusion | flops 2955476992 | bytes 15073280 | tf_op jit(solution)/shard_map/dot_general | solution.py:219
  279.3 18.7 %all_to_all.30 = bf16[4,256,512]{2,1,0:T(8,128)(2,1)S(1)} all-to-all(bf16[4,256,512]{2,1,0:T(8,128)(2,1)S(1)} %bitcast.139), channel_id=1, replica_groups=mesh['sp'=64,'tp'=4] {'tp'}, dimensions={0} | all-to-all | bytes 2097152 | tf_op jit(solution)/shard_map/all_to_all | solution.py:34
  298.1 0.2 fusion.88
  298.3 7.7 %all_to_all.31 = f32[4,1,512]{2,1,0:T(1,128)S(1)} all-to-all(f32[4,1,512]{2,1,0:T(1,128)S(1)} %broadcast_in_dim.18), channel_id=1, replica_groups=mesh['sp'=64,'tp'=4] {'tp'}, dimensions={0} | all-to-all | bytes 16384 | tf_op jit(solution)/shard_map/all_to_all | solution.py:40
  306.0 0.9 add_convert_fusion
  (53 shorter events, 1.4 us)
Async XLA Ops:
  6.5 178.8 %copy-start = (bf16[128,2048]{1,0:T(8,128)(2,1)S(1)}, bf16[128,2048]{1,0:T(8,128)(2,1)}, u32[]{:S(2)}) copy-start(bf16[128,2048]{1,0:T(8,128)(2,1)} %param.34) | copy-start | bytes 1572868
  6.5 93.4 %all-gather.4.cloned.1.call-start = ((), (), s32[]{:S(2)}) async-start(), calls=%async_computation.5 | async-start | bytes 9584640 | tf_op jit(solution)/shard_map/all_gather | solution.py:24
  9.0 231.5 %all-gather.6.cloned.1.call-start = ((), (), s32[]{:S(2)}) async-start(), calls=%async_computation.6 | async-start | bytes 11714560 | tf_op jit(solution)/shard_map/all_gather | solution.py:24
  10.7 260.2 %all-gather.8.cloned.1.call-start = ((), (), s32[]{:S(2)}) async-start(), calls=%async_computation.7 | async-start | bytes 5857280 | tf_op jit(solution)/shard_map/all_gather | solution.py:221
  110.8 8.1 %copy-start.4 = (bf16[256,64]{0,1:T(8,128)(2,1)S(1)}, bf16[256,64]{0,1:T(8,128)(2,1)}, u32[]{:S(2)}) copy-start(bf16[256,64]{0,1:T(8,128)(2,1)} %param.28) | copy-start | bytes 98308
  110.8 8.1 %copy-start.5 = (f32[256]{0:T(256)S(1)}, f32[256]{0:T(256)}, u32[]{:S(2)}) copy-start(f32[256]{0:T(256)} %param.26) | copy-start | bytes 3076
  141.4 8.2 %copy-start.3 = (bf16[256,128]{1,0:T(8,128)(2,1)S(1)}, bf16[256,128]{1,0:T(8,128)(2,1)}, u32[]{:S(2)}) copy-start(bf16[256,128]{1,0:T(8,128)(2,1)} %param.31) | copy-start | bytes 196612
  164.8 8.5 %copy-start.10 = (bf16[256,128]{1,0:T(8,128)(2,1)S(1)}, bf16[256,128]{1,0:T(8,128)(2,1)}, u32[]{:S(2)}) copy-start(bf16[256,128]{1,0:T(8,128)(2,1)} %param.32) | copy-start | bytes 196612
  173.4 12.5 %copy-start.11 = (bf16[256,64]{0,1:T(8,128)(2,1)S(1)}, bf16[256,64]{0,1:T(8,128)(2,1)}, u32[]{:S(2)}) copy-start(bf16[256,64]{0,1:T(8,128)(2,1)} %param.29) | copy-start | bytes 98308
  185.8 11.3 %copy-start.2 = (bf16[64,2048]{1,0:T(8,128)(2,1)S(1)}, bf16[64,2048]{1,0:T(8,128)(2,1)}, u32[]{:S(2)}) copy-start(bf16[64,2048]{1,0:T(8,128)(2,1)} %param.33) | copy-start | bytes 786436
  185.8 30.7 %copy-start.1 = (bf16[256,512]{1,0:T(8,128)(2,1)S(1)}, bf16[256,512]{1,0:T(8,128)(2,1)}, u32[]{:S(2)}) copy-start(bf16[256,512]{1,0:T(8,128)(2,1)} %param.21) | copy-start | bytes 786436
  197.2 27.3 %copy-start.6 = (f32[512]{0:T(512)S(1)}, f32[512]{0:T(512)}, u32[]{:S(2)}) copy-start(f32[512]{0:T(512)} %param.36) | copy-start | bytes 6148
  197.2 27.3 %copy-start.7 = (f32[512]{0:T(512)S(1)}, f32[512]{0:T(512)}, u32[]{:S(2)}) copy-start(f32[512]{0:T(512)} %param.35) | copy-start | bytes 6148
  246.1 59.9 %copy-start.8 = (f32[512]{0:T(512)S(1)}, f32[512]{0:T(512)}, u32[]{:S(2)}) copy-start(f32[512]{0:T(512)} %param.41) | copy-start | bytes 6148
  246.1 59.9 %copy-start.9 = (f32[512]{0:T(512)S(1)}, f32[512]{0:T(512)}, u32[]{:S(2)}) copy-start(f32[512]{0:T(512)} %param.40) | copy-start | bytes 6148
Sparse Core Ops, SparseCore 0:
  10.0 89.9 all-gather.3
  102.7 88.5 all-gather.5
  194.0 76.8 all-gather.7
where the time goes:
time: 314 us; the launch traced here: 313 us
  waiting for transfers between devices  110 us (35%)
  matrix products  86.3 us (27%)
  blocking collectives  68.2 us (22%)
  other arithmetic  33.7 us (11%)
  between operations  13.4 us (4%)
    all_gather x2, waiting for transfers between devices, in_one_piece(): lax.all_gather(both, axis, axis=dim, tiled=True)  84.6 us
    all_to_all x2, blocking collectives, sum_at_owner(): pieces = lax.all_to_all(split_up(x, dim, size), axis, 0, 0, tiled=True)  37.3 us
    all_to_all x3, blocking collectives, sent_to_all(): return lax.all_to_all(copies, axis, split_axis=0, concat_axis=0, tiled=True)  31 us
    dot_general x2, matrix products, update(): jnp.einsum('qhd,khd->hqk', queries[:, :, :plain_dim], key_rows, preferred...  29.5 us
    all_gather x1, waiting for transfers between devices, body(): lax.all_gather(down_weight, 'sp', axis=1, tiled=True)  24.8 us
    dot_general x2, matrix products, update(): jnp.einsum('hqk,khd->qhd', raised.astype(jnp.bfloat16), value_rows, prefe...  23.3 us
    reduce_sum x2, other arithmetic, update(): totals = totals * factor + jnp.sum(raised, axis=-1)  16.7 us
    dot_general x2, matrix products, update(): jnp.einsum('qhd,kd->hqk', queries[:, :, plain_dim:], rotary_rows, preferr...  16.2 us
  transfers between devices with their start and end apart: 3, of which 2 were waited for; matrix products, arithmetic and copies ran while one was open for 35% of the time, Pallas kernels for 0%

commit v1 on v0

--- a/solution.py
+++ b/solution.py
@@ -216,11 +216,20 @@
     gate_part = jnp.dot(full_rows, shard_rows[0], preferred_element_type=jnp.float32)
     lifted_part = jnp.dot(full_rows, shard_rows[1], preferred_element_type=jnp.float32)
     hidden = (jax.nn.silu(gate_part) * lifted_part).astype(jnp.bfloat16)
-    feed_terms = jnp.dot(
-        hidden,
-        lax.all_gather(down_weight, "sp", axis=1, tiled=True),
-        preferred_element_type=jnp.float32,
-    )
+
+    def attach_quotas(piece_in, dim_i):
+        response = jnp.concatenate(
+            jax.lax.all_to_all(
+                jnp.stack(jax.lax.axis_size("sp") * [piece_in], axis=0),
+                axis_name="sp",
+                split_axis=0,
+                concat_axis=0,
+            ),
+            dim_i,
+        )
+        return response
+
+    feed_terms = jnp.dot(hidden, attach_quotas(down_weight, 1), preferred_element_type=jnp.float32)
     feed = sum_at_owner(feed_terms.astype(jnp.bfloat16), "tp", 1)
     summed_two = DEEP_ALPHA * normed_first.astype(jnp.float32) + feed
     sums_two, squares_two = in_one(

time: 314 us -> 427 us (1.36)
  waiting for transfers between devices: 110 us -> 210 us
  starting transfers between devices: 0.09 us -> 10.9 us
    all_to_all x0 -> x1, waiting for transfers between devices: none -> 124 us  [attach_quotas(): jax.lax.all_to_all(jnp.stack(jax.lax.axis_size('sp') * [piece_in], axis=0...]
    all_gather x1 -> x0, waiting for transfers between devices: 24.8 us -> none  [body(): lax.all_gather(down_weight, 'sp', axis=1, tiled=True)]
    all_to_all x0 -> x1, starting transfers between devices: none -> 10.9 us  [attach_quotas(): jax.lax.all_to_all(jnp.stack(jax.lax.axis_size('sp') * [piece_in], axis=0...]
  transfers between devices with their start and end apart: 3 -> 3, of which waited for: 2 -> 2; matrix products, arithmetic and copies ran while one was open for 35% -> 26% of each run, Pallas kernels for 0% -> 0%
where the time goes in v1:
time: 427 us; the launch traced here: 425 us
  waiting for transfers between devices  210 us (49%)
  matrix products  86.4 us (20%)
  blocking collectives  65.5 us (15%)
  other arithmetic  33.7 us (8%)
  between operations  13.7 us (3%)
  starting transfers between devices  10.9 us (3%)
  local copies, waits for them, and re-layouts  4.48 us (1%)
    all_to_all x1, waiting for transfers between devices, attach_quotas(): jax.lax.all_to_all(jnp.stack(jax.lax.axis_size('sp') * [piece_in], axis=0...  124 us
    all_gather x2, waiting for transfers between devices, in_one_piece(): lax.all_gather(both, axis, axis=dim, tiled=True)  85.3 us
    all_to_all x2, blocking collectives, sum_at_owner(): pieces = lax.all_to_all(split_up(x, dim, size), axis, 0, 0, tiled=True)  34.3 us
    all_to_all x3, blocking collectives, sent_to_all(): return lax.all_to_all(copies, axis, split_axis=0, concat_axis=0, tiled=True)  31.2 us
    dot_general x2, matrix products, update(): jnp.einsum('qhd,khd->hqk', queries[:, :, :plain_dim], key_rows, preferred...  29.7 us
    dot_general x2, matrix products, update(): jnp.einsum('hqk,khd->qhd', raised.astype(jnp.bfloat16), value_rows, prefe...  23.2 us
    reduce_sum x2, other arithmetic, update(): totals = totals * factor + jnp.sum(raised, axis=-1)  16.7 us
    dot_general x2, matrix products, update(): jnp.einsum('qhd,kd->hqk', queries[:, :, plain_dim:], rotary_rows, preferr...  16.2 us
  transfers between devices with their start and end apart: 3, of which 2 were waited for; matrix products, arithmetic and copies ran while one was open for 26% of the time, Pallas kernels for 0%

profile of v1, /device:TPU:8, one launch (start us, length us, event | category | flops | bytes accessed | tf_op | source)
XLA Modules:
  0.0 424.6 jit_solution(5656187371803055865)
XLA Ops:
  6.5 1.1 copy.42
  7.6 1.4 pad_maximum_fusion.4
  9.1 1.6 pad_maximum_fusion.1
  10.7 1.1 fusion.72
  11.8 1.3 convolution_bitcast_fusion.4
  13.2 1.3 convolution_bitcast_fusion.5
  14.6 85.3 %all-gather.3.cloned.1.call-done = bf16[16384,288]{0,1:T(8,128)(2,1)} async-done(((bf16[256,288]{0,1:T(8,128)(2,1)}), bf16[16384,288]{0,1:T(8,128)(2,1)}) %all-gather.3.cloned.1.call-update) | async-done | bytes 9437200 | tf_op jit(solution)/shard_map/all_gather | solution.py:24
  99.9 5.1 %fusion.4 = f32[16384]{0:T(1024)S(1)} fusion(bf16[16384,288]{0,1:T(8,128)(2,1)} %all-gather.3.cloned.1.call-done), kind=kLoop, calls=%fused_computation.14 | loop fusion | flops 12566528 | bytes 8454144 | tf_op jit(solution)/shard_map/reduce_sum | solution.py:84
  105.1 1.4 fusion.62
  106.5 4.4 %fusion.84 = (bf16[16384,8]{0,1:T(8,128)(2,1)S(1)}, bf16[16384,8]{0,1:T(8,128)(2,1)S(1)}, bf16[16384,8]{0,1:T(8,128)(2,1)S(1)}, bf16[16384,8]{0,1:T(8,128)(2,1)S(1)}) fusion(f32[16384,1,32]{0,2,1:T(8,128)S(1)} %fusion.62, f32[8]{0:T(128)S(1)} %multiply_power_fusion, f32[16384]{0:T(1024)S(1)} %get-tuple-element.43, f32[16384]{0:T(1024)S(1)} %get-tuple-element.44), kind=kLoop, calls=%fused_computation.90 | loop fusion | flops 2359296 | bytes 3276832 | tf_op jit(solution)/shard_map/concatenate | solution.py:78
  110.8 8.1 %convolution_bitcast_fusion.2 = f32[1,256,16384]{2,1,0:T(8,128)} fusion(bf16[16384,8]{0,1:T(8,128)(2,1)S(1)} %get-tuple-element.13, bf16[16384,8]{0,1:T(8,128)(2,1)S(1)} %get-tuple-element.14, bf16[16384,8]{0,1:T(8,128)(2,1)S(1)} %get-tuple-element.10, bf16[16384,8]{0,1:T(8,128)(2,1)S(1)} %get-tuple-element.9, bf16[256,1,8]{0,2,1:T(8,128)(2,1)S(1)} %get-tuple-element.25, ...), kind=kOutput, calls=%fused_computation.2 | convolution fusion | flops 272695296 | bytes 17842176 | tf_op jit(solution)/shard_map/qhd,kd->hqk/dot_general | solution.py:109
  118.9 8.1 %convolution_bitcast_fusion = f32[1,256,16384]{2,1,0:T(8,128)} fusion(bf16[16384,8]{0,1:T(8,128)(2,1)S(1)} %get-tuple-element.13, bf16[16384,8]{0,1:T(8,128)(2,1)S(1)} %get-tuple-element.14, bf16[16384,8]{0,1:T(8,128)(2,1)S(1)} %get-tuple-element.10, bf16[16384,8]{0,1:T(8,128)(2,1)S(1)} %get-tuple-element.9, bf16[256,1,8]{0,2,1:T(8,128)(2,1)S(1)} %get-tuple-element.28, ...), kind=kOutput, calls=%fused_computation | convolution fusion | flops 272695296 | bytes 17842176 | tf_op jit(solution)/shard_map/qhd,kd->hqk/dot_general | solution.py:109
  127.0 14.5 %fusion.167 = (f32[256]{0:T(256)S(1)}, f32[1,256,16384]{2,1,0:T(8,128)}) fusion(f32[1,256,16384]{2,1,0:T(8,128)} %convolution_bitcast_fusion.2, bf16[256,64]{0,1:T(8,128)(2,1)S(1)} %copy-done.5, f32[256]{0:T(256)S(1)} %copy-done.6, f32[16384]{0:T(1024)S(1)} %add_rsqrt_fusion, bf16[16384,288]{0,1:T(8,128)(2,1)} %all-gather.3.cloned.1.call-done, ...), kind=kOutput, calls=%fused_computation.191 | convolution fusion | flops 1104150272 | bytes 42076160 | tf_op jit(solution)/shard_map/qhd,khd->hqk/dot_general | solution.py:106
  141.5 8.2 %fusion.7 = f32[256]{0:T(256)S(1)} fusion(f32[1,256,16384]{2,1,0:T(8,128)} %get-tuple-element.42, f32[256]{0:T(256)S(1)} %get-tuple-element.41), kind=kLoop, calls=%fused_computation.19 | loop fusion | flops 8388352 | bytes 16779264 | tf_op jit(solution)/shard_map/reduce_sum | solution.py:116
  149.7 15.2 %fusion.164 = (f32[256]{0:T(256)S(1)}, f32[1,256,16384]{2,1,0:T(8,128)}) fusion(f32[1,256,16384]{2,1,0:T(8,128)} %convolution_bitcast_fusion, bf16[256,128]{1,0:T(8,128)(2,1)S(1)} %copy-done.4, f32[256]{0:T(256)S(1)} %copy-done.6, f32[16384]{0:T(1024)S(1)} %add_rsqrt_fusion, bf16[16384,288]{0,1:T(8,128)(2,1)} %all-gather.3.cloned.1.call-done, ...), kind=kOutput, calls=%fused_computation.190 | convolution fusion | flops 2178940672 | bytes 42141696 | tf_op jit(solution)/shard_map/qhd,khd->hqk/dot_general | solution.py:106
  164.9 8.5 %fusion.9 = f32[256]{0:T(256)S(1)} fusion(f32[1,256,16384]{2,1,0:T(8,128)} %get-tuple-element.40, f32[256]{0:T(256)S(1)} %get-tuple-element.39), kind=kLoop, calls=%fused_computation.21 | loop fusion | flops 8388352 | bytes 16779264 | tf_op jit(solution)/shard_map/reduce_sum | solution.py:116
  173.4 11.9 %fusion.44 = bf16[256,128]{0,1:T(8,128)(2,1)S(1)} fusion(f32[1,256,16384]{2,1,0:T(8,128)} %get-tuple-element.40, f32[256]{0:T(256)S(1)} %get-tuple-element.39, bf16[256,128]{1,0:T(8,128)(2,1)S(1)} %copy-done.11, f32[256]{0:T(256)S(1)} %get-tuple-element.38, f32[256]{0:T(256)S(1)} %get-tuple-element.37, f32[256]{0:T(256)S(1)} %copy-done.6, ...), kind=kOutput, calls=%fused_computation.46 | convolution fusion | flops 2174844928 | bytes 25366528 | tf_op jit(solution)/shard_map/hqk,khd->qhd/dot_general | solution.py:117
  185.4 0.5 fusion.170
  185.9 11.3 %fusion.59 = bf16[256,64]{0,1:T(8,128)(2,1)S(1)} fusion(f32[1,256,16384]{2,1,0:T(8,128)} %get-tuple-element.42, f32[256]{0:T(256)S(1)} %get-tuple-element.41, bf16[256,64]{0,1:T(8,128)(2,1)S(1)} %copy-done.12, f32[256]{0:T(256)S(1)} %get-tuple-element.36, f32[256]{0:T(256)S(1)} %get-tuple-element.35, f32[256]{0:T(256)S(1)} %copy-done.6, ...), kind=kOutput, calls=%fused_computation.51 | convolution fusion | flops 1100005376 | bytes 25300992 | tf_op jit(solution)/shard_map/hqk,khd->qhd/dot_general | solution.py:117
  197.2 0.5 fusion.26
  197.8 18.7 %all_to_all.32 = bf16[4,256,512]{2,1,0:T(8,128)(2,1)S(1)} all-to-all(bf16[4,256,512]{2,1,0:T(8,128)(2,1)S(1)} %bitcast.141), channel_id=1, replica_groups=mesh['sp'=64,'tp'=4] {'tp'}, dimensions={0} | all-to-all | bytes 2097152 | tf_op jit(solution)/shard_map/all_to_all | solution.py:34
  216.6 0.2 fusion.87
  216.8 7.7 %all_to_all.33 = f32[4,1,512]{2,1,0:T(1,128)S(1)} all-to-all(f32[4,1,512]{2,1,0:T(1,128)S(1)} %broadcast_in_dim.16), channel_id=1, replica_groups=mesh['sp'=64,'tp'=4] {'tp'}, dimensions={0} | all-to-all | bytes 16384 | tf_op jit(solution)/shard_map/all_to_all | solution.py:40
  224.9 15.9 %all_to_all.34 = bf16[4,256,512]{1,2,0:T(8,128)(2,1)S(1)} all-to-all(bf16[4,256,512]{1,2,0:T(8,128)(2,1)S(1)} %broadcast_in_dim.17), channel_id=1, replica_groups=mesh['sp'=64,'tp'=4] {'tp'}, dimensions={0} | all-to-all | bytes 2097152 | tf_op jit(solution)/shard_map/all_to_all | solution.py:40
  240.8 3.0 stack.2
  243.8 10.9 %all-to-all-start.3 = ((bf16[64,1408,32]{1,2,0:T(8,128)(2,1)}), bf16[64,1408,32]{1,2,0:T(8,128)(2,1)}, u32[]{:S(2)}, u32[]{:S(2)}) async-start(bf16[64,1408,32]{1,2,0:T(8,128)(2,1)} %stack.2), calls=%async_computation.3 | async-start | bytes 11534336 | tf_op jit(solution)/shard_map/all_to_all | solution.py:222
  254.7 5.6 %fusion.21 = f32[256,1408]{1,0:T(8,128)} fusion(bf16[256,2048]{0,1:T(8,128)(2,1)S(1)} %bitcast.143, bf16[2048,2816]{1,0:T(8,128)(2,1)} %all-gather.5.cloned.1.call-done), kind=kOutput, calls=%fused_computation.31 | convolution fusion | flops 1476395008 | bytes 8257536 | tf_op jit(solution)/shard_map/dot_general | solution.py:216
  260.3 124.5 %all-to-all-done.3 = bf16[64,1408,32]{1,2,0:T(8,128)(2,1)} async-done(((bf16[64,1408,32]{1,2,0:T(8,128)(2,1)}), bf16[64,1408,32]{1,2,0:T(8,128)(2,1)}, u32[]{:S(2)}, u32[]{:S(2)}) %all-to-all-start.3) | async-done | bytes 5767200 | tf_op jit(solution)/shard_map/all_to_all | solution.py:222
  384.8 8.3 %convolution_convert_fusion.4 = bf16[256,2048]{1,0:T(8,128)(2,1)S(1)} fusion(bf16[1408,2048]{0,1:T(8,128)(2,1)} %bitcast.31, bf16[256,2048]{0,1:T(8,128)(2,1)S(1)} %bitcast.144, bf16[2048,2816]{1,0:T(8,128)(2,1)} %all-gather.5.cloned.1.call-done, f32[256,1408]{1,0:T(8,128)} %fusion.21), kind=kOutput, calls=%fused_computation.37 | convolution fusion | flops 2955476992 | bytes 15073280 | tf_op jit(solution)/shard_map/dot_general | solution.py:232
  393.2 15.6 %all_to_all.35 = bf16[4,256,512]{2,1,0:T(8,128)(2,1)S(1)} all-to-all(bf16[4,256,512]{2,1,0:T(8,128)(2,1)S(1)} %bitcast.142), channel_id=1, replica_groups=mesh['sp'=64,'tp'=4] {'tp'}, dimensions={0} | all-to-all | bytes 2097152 | tf_op jit(solution)/shard_map/all_to_all | solution.py:34
  409.2 7.7 %all_to_all.36 = f32[4,1,512]{2,1,0:T(1,128)S(1)} all-to-all(f32[4,1,512]{2,1,0:T(1,128)S(1)} %broadcast_in_dim.18), channel_id=1, replica_groups=mesh['sp'=64,'tp'=4] {'tp'}, dimensions={0} | all-to-all | bytes 16384 | tf_op jit(solution)/shard_map/all_to_all | solution.py:40
  416.9 0.9 add_convert_fusion
  (55 shorter events, 1.5 us)
Async XLA Ops:
  6.5 178.8 %copy-start = (bf16[128,2048]{1,0:T(8,128)(2,1)S(1)}, bf16[128,2048]{1,0:T(8,128)(2,1)}, u32[]{:S(2)}) copy-start(bf16[128,2048]{1,0:T(8,128)(2,1)} %param.34) | copy-start | bytes 1572868
  6.5 93.4 %all-gather.3.cloned.1.call-start = ((), (), s32[]{:S(2)}) async-start(), calls=%async_computation.6 | async-start | bytes 9584640 | tf_op jit(solution)/shard_map/all_gather | solution.py:24
  9.0 245.7 %all-gather.5.cloned.1.call-start = ((), (), s32[]{:S(2)}) async-start(), calls=%async_computation.7 | async-start | bytes 11714560 | tf_op jit(solution)/shard_map/all_gather | solution.py:24
  118.9 8.1 %copy-start.5 = (bf16[256,64]{0,1:T(8,128)(2,1)S(1)}, bf16[256,64]{0,1:T(8,128)(2,1)}, u32[]{:S(2)}) copy-start(bf16[256,64]{0,1:T(8,128)(2,1)} %param.28) | copy-start | bytes 98308
  118.9 8.1 %copy-start.6 = (f32[256]{0:T(256)S(1)}, f32[256]{0:T(256)}, u32[]{:S(2)}) copy-start(f32[256]{0:T(256)} %param.26) | copy-start | bytes 3076
  141.5 8.2 %copy-start.4 = (bf16[256,128]{1,0:T(8,128)(2,1)S(1)}, bf16[256,128]{1,0:T(8,128)(2,1)}, u32[]{:S(2)}) copy-start(bf16[256,128]{1,0:T(8,128)(2,1)} %param.31) | copy-start | bytes 196612
  164.9 8.5 %copy-start.11 = (bf16[256,128]{1,0:T(8,128)(2,1)S(1)}, bf16[256,128]{1,0:T(8,128)(2,1)}, u32[]{:S(2)}) copy-start(bf16[256,128]{1,0:T(8,128)(2,1)} %param.32) | copy-start | bytes 196612
  173.4 12.4 %copy-start.12 = (bf16[256,64]{0,1:T(8,128)(2,1)S(1)}, bf16[256,64]{0,1:T(8,128)(2,1)}, u32[]{:S(2)}) copy-start(bf16[256,64]{0,1:T(8,128)(2,1)} %param.29) | copy-start | bytes 98308
  185.8 11.3 %copy-start.2 = (bf16[64,2048]{1,0:T(8,128)(2,1)S(1)}, bf16[64,2048]{1,0:T(8,128)(2,1)}, u32[]{:S(2)}) copy-start(bf16[64,2048]{1,0:T(8,128)(2,1)} %param.33) | copy-start | bytes 786436
  185.9 30.7 %copy-start.1 = (bf16[256,512]{1,0:T(8,128)(2,1)S(1)}, bf16[256,512]{1,0:T(8,128)(2,1)}, u32[]{:S(2)}) copy-start(bf16[256,512]{1,0:T(8,128)(2,1)} %param.21) | copy-start | bytes 786436
  197.2 27.3 %copy-start.7 = (f32[512]{0:T(512)S(1)}, f32[512]{0:T(512)}, u32[]{:S(2)}) copy-start(f32[512]{0:T(512)} %param.36) | copy-start | bytes 6148
  197.2 27.3 %copy-start.8 = (f32[512]{0:T(512)S(1)}, f32[512]{0:T(512)}, u32[]{:S(2)}) copy-start(f32[512]{0:T(512)} %param.35) | copy-start | bytes 6148
  197.2 43.6 %copy-start.3 = (bf16[1408,32]{0,1:T(8,128)(2,1)S(1)}, bf16[1408,32]{0,1:T(8,128)(2,1)}, u32[]{:S(2)}) copy-start(bf16[1408,32]{0,1:T(8,128)(2,1)} %param.39) | copy-start | bytes 270340
  243.8 141.0 %all-to-all-start.3 = ((bf16[64,1408,32]{1,2,0:T(8,128)(2,1)}), bf16[64,1408,32]{1,2,0:T(8,128)(2,1)}, u32[]{:S(2)}, u32[]{:S(2)}) async-start(bf16[64,1408,32]{1,2,0:T(8,128)(2,1)} %stack.2), calls=%async_computation.3 | async-start | bytes 11534336 | tf_op jit(solution)/shard_map/all_to_all | solution.py:222
  384.8 32.1 %copy-start.9 = (f32[512]{0:T(512)S(1)}, f32[512]{0:T(512)}, u32[]{:S(2)}) copy-start(f32[512]{0:T(512)} %param.41) | copy-start | bytes 6148
  384.8 32.1 %copy-start.10 = (f32[512]{0:T(512)S(1)}, f32[512]{0:T(512)}, u32[]{:S(2)}) copy-start(f32[512]{0:T(512)} %param.40) | copy-start | bytes 6148
Sparse Core Ops, SparseCore 0:
  10.0 89.9 all-gather.2
  102.7 88.5 all-gather.4
